TPU v7x, 32 devices: a whole 2x2x4 slice. The times are simulated.
32 devices in a mesh: grp: 2 (over y), sp: 8 (over z, core), tp: 2 (over x).
Axes of the slice: x: 2, y: 2, z: 4, core: 2. Of those that a mesh axis runs over, the one named last changes fastest.
Arguments:
- query_plain: bfloat16 [2560, 1024], P(('grp', 'sp'), 'tp'), parts along dimension 0, may hold values from -6 to 6
- query_turn: bfloat16 [2560, 512], P(('grp', 'sp'), 'tp'), parts along dimension 0, may hold values from -40 to 40, as said below
- latent: bfloat16 [2560, 512], P(('grp', 'sp')), parts along dimension 0, may hold values from -6 to 6
- key_turn: bfloat16 [2560, 64], P(('grp', 'sp')), parts along dimension 0, may hold values from -40 to 40, as said below
- latent_norm_scale: bfloat16 [512], replicated, may hold values from 0.099609375 to 1.8984375
- plain_key_matrix: bfloat16 [512, 1024], P(None, 'tp'), may hold values from -0.25 to 0.25
- value_matrix: bfloat16 [512, 1024], P(None, 'tp'), may hold values from -0.25 to 0.25
- residual: bfloat16 [2560, 2048], P(('grp', 'sp', 'tp')), parts along dimension 0, may hold values from -6 to 6
- out_weight: bfloat16 [1024, 2048], replicated, may hold values from -6 to 6
- ffn_gain: bfloat16 [2048], replicated, may hold values from 0.099609375 to 1.8984375
- gate_weight: bfloat16 [8, 2048, 1024], P('sp', None, 'tp'), may hold values from -1 to 1
- up_weight: bfloat16 [8, 2048, 1024], P('sp', None, 'tp'), may hold values from -1 to 1
- down_weight: bfloat16 [8, 1024, 2048], P('sp', 'tp'), may hold values from -0.0625 to 0.0625
- routes: int32 [2560, 4], P(('grp', 'sp', 'tp')), parts along dimension 0, may hold values from 0 to 7, all different within a row; in each aligned block of 80 rows (0 to 79, 80 to 159, ...) at most 60 rows name the same one
- route_weights: float32 [2560, 4], P(('grp', 'sp', 'tp')), parts along dimension 0, may hold values from 0.1 to 0.6
Outputs:
- mixed: bfloat16 [2560, 2048], P(('grp', 'sp', 'tp')), parts along dimension 0
There are 2 independent parts, one for each index of `grp`. A program takes and returns all parts, laid end to end along the dimension named above; an argument that names none is the same for every part. Nothing has to cross between parts.
Inputs may be any that keep to these rules, and one draw needn't show every extreme that they name: `query_turn`: in the hidden draw some rows are large. `key_turn`: in the hidden draw some rows are large. `routes`: each row names 4 different experts. In each aligned block of 80 rows (the rows of one device) no expert is named more than 60 times, a bound that some block reaches.
All inputs are finite; a program needn't handle non-finite values.
Results may differ from a plain program's by a relative error of at most 0.015.
Values may be sent and summed in bfloat16 or wider, within the bound.
A program may use at most 128 MiB of HBM per device.

v0:
```python
import jax
import jax.numpy as jnp
from jax import lax
from jax.sharding import PartitionSpec as P

PLAIN_HEAD_WIDTH = 128
QK_ROPE = 64
VALUE_WIDTH = 128
GRID_W = 64
theta = 10000.0
eps = 1e-06
limit = 7.0
slope = 1.702


def turn(vector, row_shift, col_shift):
    width = vector.shape[-1]
    count = width // 4
    half = width // 2
    freqs = theta ** (-jnp.arange(count, dtype=jnp.float32) / count)
    extra = (1,) * (vector.ndim - 2)
    pieces = []
    for portion, shift in ((vector[..., :half], row_shift), (vector[..., half:], col_shift)):
        angle = (shift.astype(jnp.float32)[:, None] * freqs[None, :]).reshape(
            (shift.shape[0],) + extra + (count,)
        )
        lower = portion[..., :count]
        upper = portion[..., count:]
        pieces.append(
            jnp.concatenate(
                [
                    lower * jnp.cos(angle) - upper * jnp.sin(angle),
                    lower * jnp.sin(angle) + upper * jnp.cos(angle),
                ],
                axis=-1,
            )
        )
    return jnp.concatenate(pieces, axis=-1)


def norm_scale(values, gain):
    wide = values.astype(jnp.float32)
    return (
        wide
        * lax.rsqrt(jnp.mean(wide * wide, axis=-1, keepdims=True) + eps)
        * gain.astype(jnp.float32)
    )


def expert_active(rows, gate_w, up_w):
    gate_pre = jnp.minimum(jnp.dot(rows, gate_w, preferred_element_type=jnp.float32), limit)
    up_pre = jnp.clip(jnp.dot(rows, up_w, preferred_element_type=jnp.float32), -limit, limit)
    return ((up_pre + 1.0) * gate_pre * jax.nn.sigmoid(slope * gate_pre)).astype(jnp.bfloat16)


def expert_whole(rows, gate_w, up_w, down_w, groups):
    active = expert_active(rows, gate_w, up_w)
    piece = down_w.shape[0] // groups
    total = jnp.zeros((rows.shape[0], down_w.shape[1]), jnp.float32)
    for index in range(groups):
        product = jnp.dot(
            active[:, index * piece : (index + 1) * piece],
            down_w[index * piece : (index + 1) * piece],
            preferred_element_type=jnp.float32,
        )
        total = total + product.astype(jnp.bfloat16).astype(jnp.float32)
    return total.astype(jnp.bfloat16)


def on_device(
    query_plain,
    query_turn,
    latent,
    key_turn,
    latent_norm_scale,
    plain_key_matrix,
    value_matrix,
    residual,
    out_weight,
    ffn_gain,
    gate_weight,
    up_weight,
    down_weight,
    routes,
    route_weights,
):
    tok_dev = latent.shape[0]
    heads_dev = query_plain.shape[1] // PLAIN_HEAD_WIDTH
    model_width = residual.shape[1]
    place = lax.axis_index("sp") * tok_dev + jnp.arange(tok_dev, dtype=jnp.int32)
    grid_row = place // GRID_W
    grid_col = place % GRID_W
    normed_latent = norm_scale(latent, latent_norm_scale).astype(jnp.bfloat16)
    key_plain = jnp.dot(normed_latent, plain_key_matrix, preferred_element_type=jnp.float32).astype(
        jnp.bfloat16
    )
    values = jnp.dot(normed_latent, value_matrix, preferred_element_type=jnp.float32).astype(
        jnp.bfloat16
    )
    key_rot = turn(key_turn.astype(jnp.float32), grid_row, grid_col).astype(jnp.bfloat16)
    key_pairs = key_rot.reshape(tok_dev // 2, 2 * QK_ROPE)
    query_rot = turn(
        query_turn.astype(jnp.float32).reshape(tok_dev, heads_dev, QK_ROPE), grid_row, grid_col
    ).astype(jnp.bfloat16)
    plain_query = query_plain.reshape(tok_dev, heads_dev, PLAIN_HEAD_WIDTH)
    scale = (PLAIN_HEAD_WIDTH + QK_ROPE) ** (-0.5)
    most = jnp.full((heads_dev, tok_dev), -jnp.inf, jnp.float32)
    total = jnp.zeros((heads_dev, tok_dev), jnp.float32)
    summed = jnp.zeros((heads_dev, tok_dev, VALUE_WIDTH), jnp.float32)
    piece_keys = lax.all_gather(key_plain, "sp", axis=0, tiled=True)
    piece_values = lax.all_gather(values, "sp", axis=0, tiled=True)
    piece_pairs = lax.all_gather(key_pairs, "sp", axis=0, tiled=True)
    count = piece_keys.shape[0]
    piece_rot = piece_pairs.reshape(count, QK_ROPE)
    new_most = []
    new_total = []
    new_summed = []
    for head in range(heads_dev):
        head_keys = piece_keys[:, head * PLAIN_HEAD_WIDTH : (head + 1) * PLAIN_HEAD_WIDTH]
        head_values = piece_values[:, head * VALUE_WIDTH : (head + 1) * VALUE_WIDTH]
        scores = (
            jnp.einsum(
                "qd,kd->qk", plain_query[:, head], head_keys, preferred_element_type=jnp.float32
            )
            + jnp.einsum(
                "qd,kd->qk", query_rot[:, head], piece_rot, preferred_element_type=jnp.float32
            )
        ) * scale
        peak = jnp.max(scores, axis=1)
        factor = jnp.exp(most[head] - peak)
        weights = jnp.exp(scores - peak[:, None])
        new_total.append(total[head] * factor + jnp.sum(weights, axis=1))
        new_summed.append(
            summed[head] * factor[:, None]
            + jnp.dot(weights.astype(jnp.bfloat16), head_values, preferred_element_type=jnp.float32)
        )
        new_most.append(peak)
    total = jnp.stack(new_total)
    summed = jnp.stack(new_summed)
    attended = jnp.transpose((summed / total[..., None]).astype(jnp.bfloat16), (1, 0, 2)).reshape(
        tok_dev, heads_dev * VALUE_WIDTH
    )
    rows_dev = residual.shape[0]
    own_rows = lax.dynamic_slice_in_dim(
        out_weight, lax.axis_index("tp") * heads_dev * VALUE_WIDTH, heads_dev * VALUE_WIDTH, 0
    )
    projected = lax.psum_scatter(
        jnp.dot(attended, own_rows, preferred_element_type=jnp.float32).astype(jnp.bfloat16),
        "tp",
        scatter_dimension=0,
        tiled=True,
    ).astype(jnp.float32)
    hidden = (residual.astype(jnp.float32) + projected).astype(jnp.bfloat16)
    normed = norm_scale(hidden, ffn_gain).astype(jnp.bfloat16)
    top_count = routes.shape[1]
    experts_all = lax.axis_size("sp") * gate_weight.shape[0]
    capacity = min(rows_dev, max(2, rows_dev * top_count * 3 // (2 * experts_all)))
    flat_routes = routes.reshape(rows_dev * top_count)
    marks = (flat_routes[:, None] == jnp.arange(experts_all, dtype=jnp.int32)[None, :]).astype(
        jnp.int32
    )
    earlier = jnp.cumsum(marks, axis=0, dtype=jnp.int32) - marks
    slots = jnp.sum(earlier * marks, axis=1, dtype=jnp.int32)
    target = flat_routes * capacity + slots
    chosen = (
        target.reshape(rows_dev, top_count)[None, :, :]
        == jnp.arange(experts_all * capacity, dtype=jnp.int32)[:, None, None]
    )
    dispatch_table = jnp.sum(chosen.astype(jnp.bfloat16), axis=2)
    outgoing = jnp.dot(dispatch_table, normed, preferred_element_type=jnp.float32).astype(
        jnp.bfloat16
    )
    outgoing = outgoing.reshape(experts_all, capacity, model_width)
    gate_w = gate_weight[0]
    up_w = up_weight[0]
    down_w = down_weight[0]
    group = lax.axis_size("tp")
    gate_full, up_full, down_full = (
        lax.all_gather(gate_w, "tp", axis=1, tiled=True),
        lax.all_gather(up_w, "tp", axis=1, tiled=True),
        lax.all_gather(down_w, "tp", axis=0, tiled=True),
    )
    arrived = lax.all_to_all(outgoing, "sp", split_axis=0, concat_axis=0, tiled=True)
    result_rows = expert_whole(
        arrived.reshape(experts_all * capacity, model_width), gate_full, up_full, down_full, group
    )
    returned = lax.all_to_all(
        result_rows.reshape(experts_all, capacity, model_width),
        "sp",
        split_axis=0,
        concat_axis=0,
        tiled=True,
    )
    picked = returned.reshape(experts_all * capacity, model_width)[target]
    picked = picked.reshape(rows_dev, top_count, model_width).astype(jnp.float32)
    return (hidden.astype(jnp.float32) + jnp.sum(route_weights[..., None] * picked, axis=1)).astype(
        jnp.bfloat16
    )


def solution(mesh):
    placed = (
        P(("grp", "sp"), "tp"),
        P(("grp", "sp"), "tp"),
        P(("grp", "sp"), None),
        P(("grp", "sp"), None),
        P(),
        P(None, "tp"),
        P(None, "tp"),
        P(("grp", "sp", "tp"), None),
        P(),
        P(),
        P("sp", None, "tp"),
        P("sp", None, "tp"),
        P("sp", "tp", None),
        P(("grp", "sp", "tp"), None),
        P(("grp", "sp", "tp"), None),
    )
    return jax.shard_map(
        on_device,
        mesh=mesh,
        in_specs=placed,
        out_specs=P(("grp", "sp", "tp"), None),
        check_vma=False,
    )
```

profile of v0, /device:TPU:0, one launch (start us, length us, event | category | flops | bytes accessed | tf_op | source)
XLA Modules:
  0.0 335.4 jit_solution(11522728959038800007)
XLA Ops:
  8.4 1.9 convolution_convert_fusion.5
  10.3 2.1 convolution_convert_fusion.4
  13.1 16.3 %all_gather.19 = bf16[640,128]{1,0:T(8,128)(2,1)S(1)} all-gather(bf16[80,128]{1,0:T(8,128)(2,1)S(1)} %convert_element_type.125), channel_id=1, replica_groups=mesh['grp'=2,'sp'=8,'tp'=2] {'sp'}, dimensions={0}, use_global_device_ids=true | all-gather | bytes 184320 | tf_op jit(solution)/shard_map/all_gather | solution.py:112
  30.0 7.3 %all-gather.9.cloned.1.call-done = bf16[1280,512]{1,0:T(8,128)(2,1)} async-done(((bf16[160,512]{1,0:T(8,128)(2,1)}), bf16[1280,512]{1,0:T(8,128)(2,1)}) %all-gather.9.cloned.1.call-update) | async-done | bytes 1310736 | tf_op jit(solution)/shard_map/all_gather | solution.py:110
  43.1 18.7 %all-gather.11.cloned.1.call-done = bf16[1280,512]{1,0:T(8,128)(2,1)} async-done(((bf16[160,512]{1,0:T(8,128)(2,1)}), bf16[1280,512]{1,0:T(8,128)(2,1)}) %all-gather.11.cloned.1.call-update) | async-done | bytes 1310736 | tf_op jit(solution)/shard_map/all_gather | solution.py:111
  65.3 3.0 convolution_convert_fusion.3
  71.4 12.7 %reduce-scatter.2.cloned.1.call-done = bf16[80,2048]{1,0:T(8,128)(2,1)} async-done(((bf16[160,2048]{1,0:T(8,128)(2,1)}), bf16[80,2048]{1,0:T(8,128)(2,1)}) %reduce-scatter.2.cloned.1.call-update) | async-done | bytes 327696 | tf_op jit(solution)/shard_map/reduce_scatter | solution.py:147
  85.3 1.7 convolution_convert_fusion.2
  87.0 1.6 reshape.371
  88.6 4.6 %all-to-all-start = ((bf16[8,60,2048]{2,1,0:T(8,128)(2,1)}), bf16[8,60,2048]{2,1,0:T(8,128)(2,1)S(1)}, u32[]{:S(2)}, u32[]{:S(2)}) async-start(bf16[8,60,2048]{2,1,0:T(8,128)(2,1)} %reshape.371), calls=%async_computation.1 | async-start | bytes 4194304 | tf_op jit(solution)/shard_map/all_to_all | solution.py:183
  93.8 48.5 %all-to-all-done = bf16[8,60,2048]{2,1,0:T(8,128)(2,1)S(1)} async-done(((bf16[8,60,2048]{2,1,0:T(8,128)(2,1)}), bf16[8,60,2048]{2,1,0:T(8,128)(2,1)S(1)}, u32[]{:S(2)}, u32[]{:S(2)}) %all-to-all-start) | async-done | bytes 1966112 | tf_op jit(solution)/shard_map/all_to_all | solution.py:183
  142.2 1.5 reshape.372
  143.7 6.4 %fusion = f32[480,1024]{1,0:T(8,128)} fusion(bf16[480,2048]{1,0:T(8,128)(2,1)} %reshape.372, bf16[1,2048,1024]{2,1,0:T(8,128)(2,1)} %all-gather.15.cloned.1.call-done), kind=kOutput, calls=%fused_computation.1 | convolution fusion | flops 2013265920 | bytes 8126464 | tf_op jit(solution)/shard_map/dot_general | solution.py:51
  150.1 50.3 %all-gather.13.cloned.1.call-done = bf16[1,2048,1024]{2,1,0:T(8,128)(2,1)} async-done(((bf16[1,2048,512]{2,1,0:T(8,128)(2,1)}), bf16[1,2048,1024]{2,1,0:T(8,128)(2,1)}) %all-gather.13.cloned.1.call-update) | async-done | bytes 4194320 | tf_op jit(solution)/shard_map/all_gather | solution.py:180
  200.4 6.5 %multiply_convert_fusion = bf16[480,1024]{1,0:T(8,128)(2,1)} fusion(f32[480,1024]{1,0:T(8,128)} %fusion, bf16[480,2048]{1,0:T(8,128)(2,1)S(1)} %copy-done.5, bf16[1,2048,1024]{2,1,0:T(8,128)(2,1)} %all-gather.13.cloned.1.call-done), kind=kOutput, calls=%fused_computation.26 | convolution fusion | flops 2018181120 | bytes 9109504 | tf_op jit(solution)/shard_map/dot_general | solution.py:52
  206.9 51.7 %all-gather.17.cloned.1.call-done = bf16[1,1024,2048]{2,1,0:T(8,128)(2,1)} async-done(((bf16[1,512,2048]{2,1,0:T(8,128)(2,1)}), bf16[1,1024,2048]{2,1,0:T(8,128)(2,1)}) %all-gather.17.cloned.1.call-update) | async-done | bytes 4194320 | tf_op jit(solution)/shard_map/all_gather | solution.py:181
  258.6 3.1 convolution_convert_fusion
  263.0 1.5 reshape.373
  264.5 4.7 %all-to-all-start.1 = ((bf16[8,60,2048]{2,1,0:T(8,128)(2,1)}), bf16[8,60,2048]{2,1,0:T(8,128)(2,1)}, u32[]{:S(2)}, u32[]{:S(2)}) async-start(bf16[8,60,2048]{2,1,0:T(8,128)(2,1)} %reshape.373), calls=%async_computation.2 | async-start | bytes 4194304 | tf_op jit(solution)/shard_map/all_to_all | solution.py:187
  269.5 48.9 %all-to-all-done.1 = bf16[8,60,2048]{2,1,0:T(8,128)(2,1)} async-done(((bf16[8,60,2048]{2,1,0:T(8,128)(2,1)}), bf16[8,60,2048]{2,1,0:T(8,128)(2,1)}, u32[]{:S(2)}, u32[]{:S(2)}) %all-to-all-start.1) | async-done | bytes 1966112 | tf_op jit(solution)/shard_map/all_to_all | solution.py:187
  318.4 1.7 reshape.374
  320.1 3.0 gather_fusion
  323.2 2.6 reshape.378
  325.8 1.9 multiply_reduce_fusion
  (105 shorter events, 19.4 us)
Async XLA Ops:
  6.5 1.9 copy-start
  6.5 6.0 %copy-start.10 = (bf16[160,64]{0,1:T(8,128)(2,1)S(1)}, bf16[160,64]{0,1:T(8,128)(2,1)}, u32[]{:S(2)}) copy-start(bf16[160,64]{0,1:T(8,128)(2,1)} %param.18) | copy-start | bytes 61444
  6.5 6.0 %copy-start.9 = (bf16[160,256]{1,0:T(8,128)(2,1)S(1)}, bf16[160,256]{1,0:T(8,128)(2,1)}, u32[]{:S(2)}) copy-start(bf16[160,256]{1,0:T(8,128)(2,1)} %param.16) | copy-start | bytes 245764
  6.5 23.0 %copy-start.8 = (bf16[160,512]{1,0:T(8,128)(2,1)S(1)}, bf16[160,512]{1,0:T(8,128)(2,1)}, u32[]{:S(2)}) copy-start(bf16[160,512]{1,0:T(8,128)(2,1)} %param.15) | copy-start | bytes 491524
  6.5 30.7 %all-gather.9.cloned.1.call-start = ((), (), s32[]{:S(2)}) async-start(), calls=%async_computation.3 | async-start | bytes 1474560 | tf_op jit(solution)/shard_map/all_gather | solution.py:110
  10.3 51.6 %all-gather.11.cloned.1.call-start = ((), (), s32[]{:S(2)}) async-start(), calls=%async_computation.4 | async-start | bytes 1474560 | tf_op jit(solution)/shard_map/all_gather | solution.py:111
  12.4 71.7 %reduce-scatter.2.cloned.1.call-start = ((), (), s32[]{:S(2)}) async-start(), calls=%async_computation.5 | async-start | bytes 983040 | tf_op jit(solution)/shard_map/reduce_scatter | solution.py:147
  37.2 1.8 copy-start.6
  41.8 0.9 copy-start.1
  61.8 2.8 copy-start.7
  61.8 3.1 copy-start.2
  68.3 1.2 copy-start.12
  68.3 2.9 copy-start.11
  68.4 15.7 %copy-start.3 = (bf16[80,2048]{1,0:T(8,128)(2,1)S(1)}, bf16[80,2048]{1,0:T(8,128)(2,1)}, u32[]{:S(2)}) copy-start(bf16[80,2048]{1,0:T(8,128)(2,1)} %param.22) | copy-start | bytes 983044
  68.4 75.3 %all-gather.15.cloned.1.call-start = ((), (), s32[]{:S(2)}) async-start(), calls=%async_computation.7 | async-start | bytes 6291456 | tf_op jit(solution)/shard_map/all_gather | solution.py:179
  68.9 131.5 %all-gather.13.cloned.1.call-start = ((), (), s32[]{:S(2)}) async-start(), calls=%async_computation.6 | async-start | bytes 6291456 | tf_op jit(solution)/shard_map/all_gather | solution.py:180
  88.6 53.6 %all-to-all-start = ((bf16[8,60,2048]{2,1,0:T(8,128)(2,1)}), bf16[8,60,2048]{2,1,0:T(8,128)(2,1)S(1)}, u32[]{:S(2)}, u32[]{:S(2)}) async-start(bf16[8,60,2048]{2,1,0:T(8,128)(2,1)} %reshape.371), calls=%async_computation.1 | async-start | bytes 4194304 | tf_op jit(solution)/shard_map/all_to_all | solution.py:183
  93.2 165.4 %all-gather.17.cloned.1.call-start = ((), (), s32[]{:S(2)}) async-start(), calls=%async_computation.8 | async-start | bytes 6291456 | tf_op jit(solution)/shard_map/all_gather | solution.py:181
  143.7 56.7 %copy-start.5 = (bf16[480,2048]{1,0:T(8,128)(2,1)S(1)}, bf16[480,2048]{1,0:T(8,128)(2,1)}, u32[]{:S(2)}) copy-start(bf16[480,2048]{1,0:T(8,128)(2,1)} %reshape.372) | copy-start | bytes 5898244
  258.6 3.1 copy-start.14
  258.6 3.2 copy-start.15
  264.5 4.8 %copy-start.13 = (f32[80,4]{0,1:T(4,128)S(1)}, f32[80,4]{0,1:T(4,128)}, u32[]{:S(2)}) copy-start(f32[80,4]{0,1:T(4,128)} %param.29) | copy-start | bytes 3844
  264.5 53.9 %all-to-all-start.1 = ((bf16[8,60,2048]{2,1,0:T(8,128)(2,1)}), bf16[8,60,2048]{2,1,0:T(8,128)(2,1)}, u32[]{:S(2)}, u32[]{:S(2)}) async-start(bf16[8,60,2048]{2,1,0:T(8,128)(2,1)} %reshape.373), calls=%async_computation.2 | async-start | bytes 4194304 | tf_op jit(solution)/shard_map/all_to_all | solution.py:187
  325.8 1.9 copy-start.4
Sparse Core Ops, SparseCore 0:
  10.4 26.7 all-gather.8
  38.9 22.9 all-gather.10
  68.5 15.5 reduce-scatter.1
  85.5 56.7 all-gather.14
  143.6 56.7 all-gather.12
  201.8 56.7 all-gather.16
where the time goes:
time: 336 us; the launch traced here: 335 us
  waiting for transfers between devices  239 us (71%)
  matrix products  33 us (10%)
  blocking collectives  16.3 us (5%)
  local copies, waits for them, and re-layouts  14.6 us (4%)
  between operations  13.9 us (4%)
  starting transfers between devices  9.75 us (3%)
  other arithmetic  8.39 us (2%)
    all_gather x1, waiting for transfers between devices, on_device(): lax.all_gather(down_w, 'tp', axis=0, tiled=True)  51.7 us
    all_gather x1, waiting for transfers between devices, on_device(): lax.all_gather(up_w, 'tp', axis=1, tiled=True)  50.3 us
    all_to_all x1, waiting for transfers between devices, on_device(): lax.all_to_all(result_rows.reshape(experts_all, capacity, model_width), '...  48.9 us
    all_to_all x1, waiting for transfers between devices, on_device(): lax.all_to_all(outgoing, 'sp', split_axis=0, concat_axis=0, tiled=True)  48.5 us
    all_gather x1, waiting for transfers between devices, on_device(): piece_values = lax.all_gather(values, 'sp', axis=0, tiled=True)  18.7 us
    all_gather x1, blocking collectives, on_device(): piece_pairs = lax.all_gather(key_pairs, 'sp', axis=0, tiled=True)  16.3 us
    reduce_scatter x1, waiting for transfers between devices, on_device(): lax.psum_scatter(jnp.dot(attended, own_rows, preferred_element_type=jnp.f...  12.7 us
    all_gather x1, waiting for transfers between devices, on_device(): piece_keys = lax.all_gather(key_plain, 'sp', axis=0, tiled=True)  7.27 us
  transfers between devices with their start and end apart: 8, of which 7 were waited for; matrix products, arithmetic and copies ran while one was open for 9% of the time, Pallas kernels for 0%

commit v1 on v0

--- a/solution.py
+++ b/solution.py
@@ -11,6 +11,12 @@
 eps = 1e-06
 limit = 7.0
 slope = 1.702
+
+
+def all_parts(array, name, d):
+    parts = lax.all_gather(array, name, axis=0, tiled=False)
+    whole = jnp.concatenate(parts, axis=d)
+    return whole
 
 
 def turn(vector, row_shift, col_shift):
@@ -177,7 +183,7 @@
     group = lax.axis_size("tp")
     gate_full, up_full, down_full = (
         lax.all_gather(gate_w, "tp", axis=1, tiled=True),
-        lax.all_gather(up_w, "tp", axis=1, tiled=True),
+        all_parts(up_w, "tp", 1),
         lax.all_gather(down_w, "tp", axis=0, tiled=True),
     )
     arrived = lax.all_to_all(outgoing, "sp", split_axis=0, concat_axis=0, tiled=True)

time: 336 us -> 336 us (level)
  waiting for transfers between devices: 239 us -> 232 us
  local copies, waits for them, and re-layouts: 14.6 us -> 20.9 us
    all_to_all x1, waiting for transfers between devices: 48.5 us -> 0.01 us  [on_device(): lax.all_to_all(outgoing, 'sp', split_axis=0, concat_axis=0, tiled=True)]
    all_gather x1, waiting for transfers between devices: 0.01 us -> 43.1 us  [on_device(): lax.all_gather(gate_w, 'tp', axis=1, tiled=True)]
    all_gather x0 -> x1, local copies, waits for them, and re-layouts: none -> 6.26 us  [all_parts(): parts = lax.all_gather(array, name, axis=0, tiled=False)]
  transfers between devices with their start and end apart: 8 -> 8, of which waited for: 7 -> 7; matrix products, arithmetic and copies ran while one was open for 9% -> 11% of each run, Pallas kernels for 0% -> 0%
where the time goes in v1:
time: 336 us; the launch traced here: 335 us
  waiting for transfers between devices  232 us (69%)
  matrix products  33.9 us (10%)
  local copies, waits for them, and re-layouts  20.9 us (6%)
  blocking collectives  16.3 us (5%)
  between operations  13.9 us (4%)
  starting transfers between devices  9.75 us (3%)
  other arithmetic  8.39 us (2%)
    all_gather x1, waiting for transfers between devices, on_device(): lax.all_gather(down_w, 'tp', axis=0, tiled=True)  51.7 us
    all_to_all x1, waiting for transfers between devices, on_device(): lax.all_to_all(result_rows.reshape(experts_all, capacity, model_width), '...  48.9 us
    all_gather x1, waiting for transfers between devices, all_parts(): parts = lax.all_gather(array, name, axis=0, tiled=False)  48.5 us
    all_gather x1, waiting for transfers between devices, on_device(): lax.all_gather(gate_w, 'tp', axis=1, tiled=True)  43.1 us
    all_gather x1, waiting for transfers between devices, on_device(): piece_values = lax.all_gather(values, 'sp', axis=0, tiled=True)  18.7 us
    all_gather x1, blocking collectives, on_device(): piece_pairs = lax.all_gather(key_pairs, 'sp', axis=0, tiled=True)  16.3 us
    reduce_scatter x1, waiting for transfers between devices, on_device(): lax.psum_scatter(jnp.dot(attended, own_rows, preferred_element_type=jnp.f...  12.7 us
    dot_general x1, matrix products, expert_active(): jnp.dot(rows, up_w, preferred_element_type=jnp.float32)  7.32 us
  transfers between devices with their start and end apart: 8, of which 7 were waited for; matrix products, arithmetic and copies ran while one was open for 11% of the time, Pallas kernels for 0%

profile of v1, /device:TPU:0, one launch (start us, length us, event | category | flops | bytes accessed | tf_op | source)
XLA Modules:
  0.0 335.5 jit_solution(4428656727196875114)
XLA Ops:
  8.4 1.9 convolution_convert_fusion.5
  10.3 2.1 convolution_convert_fusion.4
  13.1 16.3 %all_gather.19 = bf16[640,128]{1,0:T(8,128)(2,1)S(1)} all-gather(bf16[80,128]{1,0:T(8,128)(2,1)S(1)} %convert_element_type.125), channel_id=1, replica_groups=mesh['grp'=2,'sp'=8,'tp'=2] {'sp'}, dimensions={0}, use_global_device_ids=true | all-gather | bytes 184320 | tf_op jit(solution)/shard_map/all_gather | solution.py:118
  30.0 7.3 %all-gather.8.cloned.1.call-done = bf16[1280,512]{1,0:T(8,128)(2,1)} async-done(((bf16[160,512]{1,0:T(8,128)(2,1)}), bf16[1280,512]{1,0:T(8,128)(2,1)}) %all-gather.8.cloned.1.call-update) | async-done | bytes 1310736 | tf_op jit(solution)/shard_map/all_gather | solution.py:116
  43.1 18.7 %all-gather.10.cloned.1.call-done = bf16[1280,512]{1,0:T(8,128)(2,1)} async-done(((bf16[160,512]{1,0:T(8,128)(2,1)}), bf16[1280,512]{1,0:T(8,128)(2,1)}) %all-gather.10.cloned.1.call-update) | async-done | bytes 1310736 | tf_op jit(solution)/shard_map/all_gather | solution.py:117
  65.3 3.0 convolution_convert_fusion.3
  71.4 12.7 %reduce-scatter.2.cloned.1.call-done = bf16[80,2048]{1,0:T(8,128)(2,1)} async-done(((bf16[160,2048]{1,0:T(8,128)(2,1)}), bf16[80,2048]{1,0:T(8,128)(2,1)}) %reduce-scatter.2.cloned.1.call-update) | async-done | bytes 327696 | tf_op jit(solution)/shard_map/reduce_scatter | solution.py:153
  85.3 1.7 convolution_convert_fusion.2
  87.0 1.6 reshape.377
  88.6 4.6 %all-to-all-start = ((bf16[8,60,2048]{2,1,0:T(8,128)(2,1)}), bf16[8,60,2048]{2,1,0:T(8,128)(2,1)S(1)}, u32[]{:S(2)}, u32[]{:S(2)}) async-start(bf16[8,60,2048]{2,1,0:T(8,128)(2,1)} %reshape.377), calls=%async_computation.1 | async-start | bytes 4194304 | tf_op jit(solution)/shard_map/all_to_all | solution.py:189
  93.7 48.5 %all-gather.12.cloned.1.call-done = bf16[2,2048,512]{2,1,0:T(8,128)(2,1)} async-done(((bf16[1,2048,512]{2,1,0:T(8,128)(2,1)}), bf16[2,2048,512]{2,1,0:T(8,128)(2,1)}) %all-gather.12.cloned.1.call-update) | async-done | bytes 4194320 | tf_op jit(solution)/shard_map/all_gather | solution.py:17
  142.2 6.3 %copy.50 = bf16[2,2048,512]{1,2,0:T(8,128)(2,1)} copy(bf16[2,2048,512]{2,1,0:T(8,128)(2,1)} %all-gather.12.cloned.1.call-done) | data formatting | bytes 8388608 | tf_op jit(solution)/shard_map/all_gather | solution.py:17
  150.0 7.3 %fusion.82 = f32[480,1024]{1,0:T(8,128)} fusion(bf16[480,2048]{1,0:T(8,128)(2,1)} %reshape.378, bf16[2048,1024]{0,1:T(8,128)(2,1)} %bitcast.93), kind=kOutput, calls=%fused_computation.151 | convolution fusion | flops 2013265920 | bytes 8126464 | tf_op jit(solution)/shard_map/dot_general | solution.py:58
  157.3 43.1 %all-gather.14.cloned.1.call-done = bf16[1,2048,1024]{2,1,0:T(8,128)(2,1)} async-done(((bf16[1,2048,512]{2,1,0:T(8,128)(2,1)}), bf16[1,2048,1024]{2,1,0:T(8,128)(2,1)}) %all-gather.14.cloned.1.call-update) | async-done | bytes 4194320 | tf_op jit(solution)/shard_map/all_gather | solution.py:185
  200.4 6.4 %multiply_convert_fusion = bf16[480,1024]{1,0:T(8,128)(2,1)} fusion(f32[480,1024]{1,0:T(8,128)} %fusion.82, bf16[480,2048]{1,0:T(8,128)(2,1)S(1)} %copy-done.6, bf16[1,2048,1024]{2,1,0:T(8,128)(2,1)} %all-gather.14.cloned.1.call-done), kind=kOutput, calls=%fused_computation.24 | convolution fusion | flops 2018181120 | bytes 9109504 | tf_op jit(solution)/shard_map/dot_general | solution.py:57
  206.8 51.7 %all-gather.16.cloned.1.call-done = bf16[1,1024,2048]{2,1,0:T(8,128)(2,1)} async-done(((bf16[1,512,2048]{2,1,0:T(8,128)(2,1)}), bf16[1,1024,2048]{2,1,0:T(8,128)(2,1)}) %all-gather.16.cloned.1.call-update) | async-done | bytes 4194320 | tf_op jit(solution)/shard_map/all_gather | solution.py:187
  258.6 3.1 convolution_convert_fusion
  263.0 1.5 reshape.381
  264.5 4.7 %all-to-all-start.1 = ((bf16[8,60,2048]{2,1,0:T(8,128)(2,1)}), bf16[8,60,2048]{2,1,0:T(8,128)(2,1)}, u32[]{:S(2)}, u32[]{:S(2)}) async-start(bf16[8,60,2048]{2,1,0:T(8,128)(2,1)} %reshape.381), calls=%async_computation.2 | async-start | bytes 4194304 | tf_op jit(solution)/shard_map/all_to_all | solution.py:193
  269.5 48.9 %all-to-all-done.1 = bf16[8,60,2048]{2,1,0:T(8,128)(2,1)} async-done(((bf16[8,60,2048]{2,1,0:T(8,128)(2,1)}), bf16[8,60,2048]{2,1,0:T(8,128)(2,1)}, u32[]{:S(2)}, u32[]{:S(2)}) %all-to-all-start.1) | async-done | bytes 1966112 | tf_op jit(solution)/shard_map/all_to_all | solution.py:193
  318.4 1.7 reshape.382
  320.1 3.0 gather_fusion
  323.2 2.7 reshape.386
  325.9 1.9 multiply_reduce_fusion
  (108 shorter events, 20.8 us)
Async XLA Ops:
  6.5 1.9 copy-start
  6.5 6.0 %copy-start.11 = (bf16[160,64]{0,1:T(8,128)(2,1)S(1)}, bf16[160,64]{0,1:T(8,128)(2,1)}, u32[]{:S(2)}) copy-start(bf16[160,64]{0,1:T(8,128)(2,1)} %param.18) | copy-start | bytes 61444
  6.5 6.0 %copy-start.10 = (bf16[160,256]{1,0:T(8,128)(2,1)S(1)}, bf16[160,256]{1,0:T(8,128)(2,1)}, u32[]{:S(2)}) copy-start(bf16[160,256]{1,0:T(8,128)(2,1)} %param.16) | copy-start | bytes 245764
  6.5 23.0 %copy-start.9 = (bf16[160,512]{1,0:T(8,128)(2,1)S(1)}, bf16[160,512]{1,0:T(8,128)(2,1)}, u32[]{:S(2)}) copy-start(bf16[160,512]{1,0:T(8,128)(2,1)} %param.15) | copy-start | bytes 491524
  6.5 30.7 %all-gather.8.cloned.1.call-start = ((), (), s32[]{:S(2)}) async-start(), calls=%async_computation.3 | async-start | bytes 1474560 | tf_op jit(solution)/shard_map/all_gather | solution.py:116
  10.3 51.6 %all-gather.10.cloned.1.call-start = ((), (), s32[]{:S(2)}) async-start(), calls=%async_computation.4 | async-start | bytes 1474560 | tf_op jit(solution)/shard_map/all_gather | solution.py:117
  12.4 71.7 %reduce-scatter.2.cloned.1.call-start = ((), (), s32[]{:S(2)}) async-start(), calls=%async_computation.5 | async-start | bytes 983040 | tf_op jit(solution)/shard_map/reduce_scatter | solution.py:153
  37.2 1.8 copy-start.7
  61.8 2.8 copy-start.8
  61.8 3.1 copy-start.3
  68.3 1.2 copy-start.13
  68.3 2.9 copy-start.12
  68.4 15.7 %copy-start.4 = (bf16[80,2048]{1,0:T(8,128)(2,1)S(1)}, bf16[80,2048]{1,0:T(8,128)(2,1)}, u32[]{:S(2)}) copy-start(bf16[80,2048]{1,0:T(8,128)(2,1)} %param.22) | copy-start | bytes 983044
  68.4 73.9 %all-gather.12.cloned.1.call-start = ((), (), s32[]{:S(2)}) async-start(), calls=%async_computation.6 | async-start | bytes 6291456 | tf_op jit(solution)/shard_map/all_gather | solution.py:17
  68.9 131.4 %all-gather.14.cloned.1.call-start = ((), (), s32[]{:S(2)}) async-start(), calls=%async_computation.7 | async-start | bytes 6291456 | tf_op jit(solution)/shard_map/all_gather | solution.py:185
  88.6 59.9 %all-to-all-start = ((bf16[8,60,2048]{2,1,0:T(8,128)(2,1)}), bf16[8,60,2048]{2,1,0:T(8,128)(2,1)S(1)}, u32[]{:S(2)}, u32[]{:S(2)}) async-start(bf16[8,60,2048]{2,1,0:T(8,128)(2,1)} %reshape.377), calls=%async_computation.1 | async-start | bytes 4194304 | tf_op jit(solution)/shard_map/all_to_all | solution.py:189
  93.2 165.4 %all-gather.16.cloned.1.call-start = ((), (), s32[]{:S(2)}) async-start(), calls=%async_computation.8 | async-start | bytes 6291456 | tf_op jit(solution)/shard_map/all_gather | solution.py:187
  150.0 50.4 %copy-start.6 = (bf16[480,2048]{1,0:T(8,128)(2,1)S(1)}, bf16[480,2048]{1,0:T(8,128)(2,1)}, u32[]{:S(2)}) copy-start(bf16[480,2048]{1,0:T(8,128)(2,1)} %reshape.378) | copy-start | bytes 5898244
  258.6 3.1 copy-start.15
  258.6 3.2 copy-start.16
  264.5 4.8 %copy-start.14 = (f32[80,4]{0,1:T(4,128)S(1)}, f32[80,4]{0,1:T(4,128)}, u32[]{:S(2)}) copy-start(f32[80,4]{0,1:T(4,128)} %param.29) | copy-start | bytes 3844
  264.5 53.9 %all-to-all-start.1 = ((bf16[8,60,2048]{2,1,0:T(8,128)(2,1)}), bf16[8,60,2048]{2,1,0:T(8,128)(2,1)}, u32[]{:S(2)}, u32[]{:S(2)}) async-start(bf16[8,60,2048]{2,1,0:T(8,128)(2,1)} %reshape.381), calls=%async_computation.2 | async-start | bytes 4194304 | tf_op jit(solution)/shard_map/all_to_all | solution.py:193
  323.2 5.5 %copy-start.1 = (bf16[512,512]{1,0:T(8,128)(2,1)S(1)}, bf16[512,512]{1,0:T(8,128)(2,1)}, u32[]{:S(2)}) copy-start(bf16[512,512]{1,0:T(8,128)(2,1)} %param.20) | copy-start | bytes 1572868
  325.8 1.9 copy-start.5
  (1 other events, 0.9 us)
Sparse Core Ops, SparseCore 0:
  10.4 26.7 all-gather.7
  38.9 22.9 all-gather.9
  68.5 15.5 reduce-scatter.1
  85.5 56.7 all-gather.11
  143.6 56.7 all-gather.13
  201.8 56.7 all-gather.15
